TPU v7x, 32 devices: a whole 2x2x4 slice. The times are simulated.
32 devices in a mesh: sp: 8 (over z, y), tp: 4 (over x, core).
Axes of the slice: x: 2, y: 2, z: 4, core: 2. Of those that a mesh axis runs over, the one named last changes fastest.
Arguments:
- prompt_input: bfloat16 [2304, 2048], P('sp'), may hold values from -6 to 6
- next_input: bfloat16 [2048], replicated, may hold values from -6 to 6
- norm_gain: float32 [2048], replicated, may hold values from 0.1 to 1.9
- w_key: bfloat16 [2048, 1024], P(None, 'tp'), may hold values from -0.125 to 0.125
- w_value: bfloat16 [2048, 1024], P(None, 'tp'), may hold values from -0.125 to 0.125
- w_query: bfloat16 [2048, 1024], P(None, 'tp'), may hold values from -0.125 to 0.125
- key_offset: float32 [2304, 8], P('sp', 'tp'), may hold values from -10 to 0, as said below
Outputs:
- key_cache: bfloat16 [8, 8, 36, 1024], P('sp', None, None, 'tp')
- value_cache: bfloat16 [8, 8, 36, 1024], P('sp', None, None, 'tp')
- reading: bfloat16 [1024], replicated
Inputs may be any that keep to these rules, and one draw needn't show every extreme that they name: `key_offset`: finite log-odds offsets, one per key and head.
All inputs are finite; a program needn't handle non-finite values.
Results may differ from a plain program's by a relative error of at most 0.011.
Values may be sent and summed in bfloat16 or wider, within the bound.
A program may use at most 64 MiB of HBM per device.

v0:
```python
import jax
import jax.numpy as jnp
from jax import lax
from jax.sharding import PartitionSpec as P

HEAD_DIM = 128


def norm_rows(row_block, gain_vec):
    wide_rows = row_block.astype(jnp.float32)
    inv_rms = lax.rsqrt(jnp.mean(wide_rows * wide_rows, axis=-1, keepdims=True) + 1e-06)
    return (wide_rows * inv_rms * gain_vec).astype(jnp.bfloat16)


def shards(prompt_input, next_input, norm_gain, w_key, w_value, w_query, key_offset):
    span_len = prompt_input.shape[0]
    head_width = w_key.shape[1]
    heads_here = head_width // HEAD_DIM
    score_scale = HEAD_DIM ** (-0.5)
    slots = lax.axis_size("sp")
    sub_len = span_len // slots
    normed = norm_rows(prompt_input, norm_gain)
    key_rows = jnp.dot(normed, w_key, preferred_element_type=jnp.float32).astype(jnp.bfloat16)
    value_rows = jnp.dot(normed, w_value, preferred_element_type=jnp.float32).astype(jnp.bfloat16)
    outgoing = jnp.stack([key_rows, value_rows]).reshape(2, slots, 1, sub_len, head_width)
    arrived = lax.all_to_all(outgoing, "sp", split_axis=1, concat_axis=2, tiled=True)
    key_cache = arrived[0]
    value_cache = arrived[1]
    new_query = jnp.dot(
        norm_rows(next_input[None, :], norm_gain), w_query, preferred_element_type=jnp.float32
    )
    new_query = new_query.astype(jnp.bfloat16).reshape(heads_here, HEAD_DIM)
    key_heads = key_rows.reshape(span_len, heads_here, HEAD_DIM)
    value_heads = value_rows.reshape(span_len, heads_here, HEAD_DIM)
    logits = (
        jnp.einsum("hd,shd->sh", new_query, key_heads, preferred_element_type=jnp.float32)
        * score_scale
        + key_offset
    )
    log_breaks = jax.nn.log_sigmoid(-logits)
    inner_sum = lax.cumsum(log_breaks, axis=0, reverse=True) - log_breaks
    block_totals = jnp.sum(log_breaks, axis=0)
    every_total = lax.all_gather(block_totals[None], "sp", axis=0, tiled=True)
    block_ids = lax.broadcasted_iota(jnp.int32, every_total.shape, 0)
    carried = jnp.sum(jnp.where(block_ids > lax.axis_index("sp"), every_total, 0.0), axis=0)
    weights = jnp.exp(jax.nn.log_sigmoid(logits) + inner_sum + carried[None, :])
    partial_value = jnp.einsum("sh,shd->hd", weights, value_heads.astype(jnp.float32))
    summed = lax.psum(partial_value, "sp")
    own_read = summed.reshape(head_width).astype(jnp.bfloat16)
    reading = lax.all_gather(own_read, "tp", axis=0, tiled=True)
    return (key_cache, value_cache, reading)


def solution(mesh):
    placed = (P("sp", None), P(), P(), P(None, "tp"), P(None, "tp"), P(None, "tp"), P("sp", "tp"))
    return jax.shard_map(
        shards,
        mesh=mesh,
        in_specs=placed,
        out_specs=(P("sp", None, None, "tp"), P("sp", None, None, "tp"), P()),
        check_vma=False,
    )
```

profile of v0, /device:TPU:0, one launch (start us, length us, event | category | flops | bytes accessed | tf_op | source)
XLA Modules:
  0.0 65.4 jit_solution(9334492287471043287)
XLA Ops:
  0.6 0.0 copy-start
  0.6 0.0 copy-start.1
  0.7 1.7 %fusion = f32[288]{0:T(512)S(1)} fusion(bf16[288,2048]{1,0:T(8,128)(2,1)} %param.7), kind=kLoop, calls=%fused_computation.2 | loop fusion | flops 1769184 | bytes 1180800 | tf_op jit(solution)/shard_map/reduce_sum | solution.py:11
  2.4 0.0 copy-done
  2.4 0.2 copy-done.1
  2.6 0.0 copy-start.5
  2.6 0.0 copy-start.6
  2.6 1.3 %convolution_convert_fusion = bf16[288,256]{1,0:T(8,128)(2,1)S(1)} fusion(bf16[2048,256]{1,0:T(8,128)(2,1)S(1)} %copy-done, bf16[288,2048]{1,0:T(8,128)(2,1)S(1)} %copy-done.1, f32[2048]{0:T(1024)} %param.9, f32[288]{0:T(512)S(1)} %add_rsqrt_fusion), kind=kOutput, calls=%fused_computation.5 | convolution fusion | flops 304422912 | bytes 2385024 | tf_op jit(solution)/shard_map/dot_general | solution.py:24
  3.9 0.0 copy-done.5
  3.9 0.0 copy-done.6
  3.9 0.5 convolution_convert_fusion.1
  4.5 0.0 copy-start.3
  4.5 0.0 copy-start.2
  4.6 0.0 copy-start.7
  4.6 0.0 copy-start.4
  4.6 1.0 %copy.17 = bf16[2,8,1,36,256]{4,0,3,2,1:T(2,128)(2,1)} copy(bf16[2,8,1,36,256]{4,3,1,2,0:T(8,128)(2,1)S(1)} %pad_maximum_fusion) | data formatting | bytes 589824 | tf_op jit(solution)/shard_map/stack | solution.py:25
  5.6 7.3 %all-to-all-start = ((bf16[2,8,1,36,256]{4,0,3,2,1:T(2,128)(2,1)}), bf16[2,8,1,36,256]{4,0,3,2,1:T(2,128)(2,1)S(1)}, u32[]{:S(2)}, u32[]{:S(2)}) async-start(bf16[2,8,1,36,256]{4,0,3,2,1:T(2,128)(2,1)} %copy.17), calls=%async_computation | async-start | bytes 589824 | tf_op jit(solution)/shard_map/all_to_all | solution.py:26
  13.0 0.0 copy-done.3
  13.0 0.6 fusion.11
  14.3 0.0 copy-done.2
  14.3 0.2 fusion.21
  14.5 0.1 fusion.8
  14.7 0.0 copy-done.7
  14.7 0.6 dynamic-slice
  16.0 0.0 copy-done.4
  16.0 0.1 fusion.19
  16.1 0.1 negate_dynamic-update-slice_fusion
  16.2 21.8 %all-reduce.1 = f32[16]{0:T(128)S(1)} all-reduce(f32[16]{0:T(128)S(1)} %negate_dynamic-update-slice_fusion), channel_id=2, replica_groups=mesh['sp'=8,'tp'=4] {'sp'}, use_global_device_ids=true, to_apply=%add.1 | all-reduce | flops 16 | bytes 128
  38.1 2.5 %reduce-window.6 = f32[2,3,128]{2,1,0:T(4,128)S(1)} reduce-window(f32[2,3,128]{2,1,0:T(4,128)S(1)} %reshape.81, f32[]{:T(128)} %constant.20.clone.1), window={size=1x1x128 pad=0_0x0_0x0_127}, to_apply=%region_2.3 | reduce-window | flops 97536 | bytes 6148 | tf_op jit(solution)/shard_map/reduce-window
  40.6 0.1 slice_reduce_fusion
  40.7 0.2 reduce-window.9
  40.9 0.1 slice.21
  40.9 0.1 add_bitcast_fusion
  41.0 0.1 reshape.84
  41.1 0.1 select_reduce_fusion
  41.2 0.1 exponential_bitcast_fusion
  41.3 0.1 fusion.5
  41.4 17.1 %psum.7 = bf16[2,128]{1,0:T(2,128)(2,1)S(1)} all-reduce(f32[2,128]{1,0:T(2,128)S(1)} %bitcast.64), channel_id=1, replica_groups=mesh['sp'=8,'tp'=4] {'sp'}, use_global_device_ids=true, to_apply=%region_6.7 | all-reduce | flops 256 | bytes 1536 | tf_op jit(solution)/shard_map/psum | solution.py:48
  58.6 5.1 %all-gather.1 = bf16[4,1,256]{2,1,0:T(2,128)(2,1)S(1)} all-gather(bf16[1,1,256]{2,1,0:T(2,128)(2,1)S(1)} %reshape.88), channel_id=1, replica_groups=mesh['sp'=8,'tp'=4] {'tp'}, dimensions={0}, use_global_device_ids=true | all-gather | bytes 2560 | tf_op jit(solution)/shard_map/all_gather | solution.py:50
  63.6 0.6 copy.31
  64.2 0.0 all-to-all-done
  64.2 0.4 fusion.20
  64.6 0.8 %copy_bitcast_fusion = (bf16[1,8,36,256]{3,1,2,0:T(8,128)(2,1)}, bf16[1,8,36,256]{3,1,2,0:T(8,128)(2,1)}) fusion(bf16[1,8,1,36,256]{4,0,3,2,1:T(2,128)(2,1)S(1)} %get-tuple-element.11, bf16[1,8,1,36,256]{4,0,3,2,1:T(2,128)(2,1)S(1)} %get-tuple-element.12), kind=kLoop, calls=%fused_computation.14 | loop fusion | bytes 589824 | tf_op jit(solution)/shard_map/squeeze | solution.py:28
  (15 shorter events, 0.2 us)
Async XLA Ops:
  0.6 1.8 %copy-start = (bf16[2048,256]{1,0:T(8,128)(2,1)S(1)}, bf16[2048,256]{1,0:T(8,128)(2,1)}, u32[]{:S(2)}) copy-start(bf16[2048,256]{1,0:T(8,128)(2,1)} %param.11) | copy-start | bytes 3145732
  0.6 1.9 %copy-start.1 = (bf16[288,2048]{1,0:T(8,128)(2,1)S(1)}, bf16[288,2048]{1,0:T(8,128)(2,1)}, u32[]{:S(2)}) copy-start(bf16[288,2048]{1,0:T(8,128)(2,1)} %param.7) | copy-start | bytes 3538948
  2.6 1.3 %copy-start.5 = (f32[2048]{0:T(1024)S(1)}, f32[2048]{0:T(1024)}, u32[]{:S(2)}) copy-start(f32[2048]{0:T(1024)} %param.9) | copy-start | bytes 24580
  2.6 1.3 %copy-start.6 = (bf16[2048,256]{1,0:T(8,128)(2,1)S(1)}, bf16[2048,256]{1,0:T(8,128)(2,1)}, u32[]{:S(2)}) copy-start(bf16[2048,256]{1,0:T(8,128)(2,1)} %param.10) | copy-start | bytes 3145732
  4.5 8.5 %copy-start.3 = (bf16[2048]{0:T(1024)(128)(2,1)S(1)}, bf16[2048]{0:T(1024)(128)(2,1)}, u32[]{:S(2)}) copy-start(bf16[2048]{0:T(1024)(128)(2,1)} %param.8) | copy-start | bytes 12292
  4.5 9.8 %copy-start.2 = (bf16[2048,256]{1,0:T(8,128)(2,1)S(1)}, bf16[2048,256]{1,0:T(8,128)(2,1)}, u32[]{:S(2)}) copy-start(bf16[2048,256]{1,0:T(8,128)(2,1)} %param.12) | copy-start | bytes 3145732
  4.6 10.1 %copy-start.7 = (u32[32]{0:T(128)S(1)}, u32[32]{0:T(128)}, u32[]{:S(2)}) copy-start(u32[32]{0:T(128)} %constant.31) | copy-start | bytes 388
  4.6 11.3 %copy-start.4 = (f32[288,2]{0,1:T(2,128)S(1)}, f32[288,2]{0,1:T(2,128)}, u32[]{:S(2)}) copy-start(f32[288,2]{0,1:T(2,128)} %param.13) | copy-start | bytes 6916
  5.6 58.6 %all-to-all-start = ((bf16[2,8,1,36,256]{4,0,3,2,1:T(2,128)(2,1)}), bf16[2,8,1,36,256]{4,0,3,2,1:T(2,128)(2,1)S(1)}, u32[]{:S(2)}, u32[]{:S(2)}) async-start(bf16[2,8,1,36,256]{4,0,3,2,1:T(2,128)(2,1)} %copy.17), calls=%async_computation | async-start | bytes 589824 | tf_op jit(solution)/shard_map/all_to_all | solution.py:26
where the time goes:
time: 65.7 us; the launch traced here: 65.4 us
  blocking collectives  44 us (67%)
  starting transfers between devices  7.31 us (11%)
  other arithmetic  5.61 us (9%)
  local copies, waits for them, and re-layouts  3.98 us (6%)
  matrix products  2.36 us (4%)
  between operations  2.15 us (3%)
    unnamed x1, blocking collectives  21.8 us
    psum x1, blocking collectives, shards(): summed = lax.psum(partial_value, 'sp')  17.1 us
    all_to_all x1, starting transfers between devices, shards(): lax.all_to_all(outgoing, 'sp', split_axis=1, concat_axis=2, tiled=True)  7.31 us
    all_gather x1, blocking collectives, shards(): reading = lax.all_gather(own_read, 'tp', axis=0, tiled=True)  5.05 us
    another operation x2, other arithmetic  2.71 us
    reduce_sum x2, other arithmetic, norm_rows(): jnp.mean(wide_rows * wide_rows, axis=-1, keepdims=True) + 1e-06  2.34 us
    unnamed x21, local copies, waits for them, and re-layouts  1.43 us
  transfers between devices with their start and end apart: 1, of which 0 were waited for; matrix products, arithmetic and copies ran while one was open for 9% of the time, Pallas kernels for 0%

commit v1 on v0

--- a/solution.py
+++ b/solution.py
@@ -47,7 +47,13 @@
     partial_value = jnp.einsum("sh,shd->hd", weights, value_heads.astype(jnp.float32))
     summed = lax.psum(partial_value, "sp")
     own_read = summed.reshape(head_width).astype(jnp.bfloat16)
-    reading = lax.all_gather(own_read, "tp", axis=0, tiled=True)
+    size = lax.axis_size("tp")
+    held, blocks = (own_read, [own_read])
+    for _ in range(size - 1):
+        held = lax.ppermute(held, "tp", [(i, (i + 1) % size) for i in range(size)])
+        blocks.insert(0, held)
+    flat = jnp.concatenate(blocks, axis=0)
+    reading = jnp.roll(flat, (lax.axis_index("tp") + 1) * own_read.shape[0], axis=0)
     return (key_cache, value_cache, reading)
 
 

time: 65.7 us -> 71.3 us (1.085)
  waiting for transfers between devices: 0.01 us -> 8.96 us
  blocking collectives: 44 us -> 39 us
  local copies, waits for them, and re-layouts: 3.98 us -> 5.61 us
    ppermute x0 -> x3, waiting for transfers between devices: none -> 8.96 us  [shards(): held = lax.ppermute(held, 'tp', [(i, (i + 1) % size) for i in range(size)])]
    all_gather x1 -> x0, blocking collectives: 5.05 us -> none  [shards(): reading = lax.all_gather(own_read, 'tp', axis=0, tiled=True)]
    unnamed x21 -> x26, local copies, waits for them, and re-layouts: 1.43 us -> 2.2 us
  transfers between devices with their start and end apart: 1 -> 4, of which waited for: 0 -> 3; matrix products, arithmetic and copies ran while one was open for 9% -> 10% of each run, Pallas kernels for 0% -> 0%
where the time goes in v1:
time: 71.3 us; the launch traced here: 71 us
  blocking collectives  39 us (55%)
  waiting for transfers between devices  8.96 us (13%)
  starting transfers between devices  7.35 us (10%)
  local copies, waits for them, and re-layouts  5.61 us (8%)
  other arithmetic  5.59 us (8%)
  matrix products  2.36 us (3%)
  between operations  2.17 us (3%)
    unnamed x1, blocking collectives  21.8 us
    psum x1, blocking collectives, shards(): summed = lax.psum(partial_value, 'sp')  17.1 us
    ppermute x3, waiting for transfers between devices, shards(): held = lax.ppermute(held, 'tp', [(i, (i + 1) % size) for i in range(size)])  8.96 us
    all_to_all x1, starting transfers between devices, shards(): lax.all_to_all(outgoing, 'sp', split_axis=1, concat_axis=2, tiled=True)  7.31 us
    another operation x2, other arithmetic  2.71 us
    reduce_sum x2, other arithmetic, norm_rows(): jnp.mean(wide_rows * wide_rows, axis=-1, keepdims=True) + 1e-06  2.34 us
    unnamed x26, local copies, waits for them, and re-layouts  2.2 us
  transfers between devices with their start and end apart: 4, of which 3 were waited for; matrix products, arithmetic and copies ran while one was open for 10% of the time, Pallas kernels for 0%

profile of v1, /device:TPU:0, one launch (start us, length us, event | category | flops | bytes accessed | tf_op | source)
XLA Modules:
  0.0 71.0 jit_solution(10630098266762559142)
XLA Ops:
  0.6 0.0 copy-start
  0.6 0.0 copy-start.1
  0.7 1.7 %fusion = f32[288]{0:T(512)S(1)} fusion(bf16[288,2048]{1,0:T(8,128)(2,1)} %param.7), kind=kLoop, calls=%fused_computation.2 | loop fusion | flops 1769184 | bytes 1180800 | tf_op jit(solution)/shard_map/reduce_sum | solution.py:11
  2.4 0.0 copy-done
  2.4 0.2 copy-done.1
  2.6 0.0 copy-start.5
  2.6 0.0 copy-start.6
  2.6 1.3 %convolution_convert_fusion = bf16[288,256]{1,0:T(8,128)(2,1)S(1)} fusion(bf16[2048,256]{1,0:T(8,128)(2,1)S(1)} %copy-done, bf16[288,2048]{1,0:T(8,128)(2,1)S(1)} %copy-done.1, f32[2048]{0:T(1024)} %param.9, f32[288]{0:T(512)S(1)} %add_rsqrt_fusion), kind=kOutput, calls=%fused_computation.5 | convolution fusion | flops 304422912 | bytes 2385024 | tf_op jit(solution)/shard_map/dot_general | solution.py:24
  3.9 0.0 copy-done.5
  3.9 0.0 copy-done.6
  3.9 0.5 convolution_convert_fusion.1
  4.5 0.0 copy-start.3
  4.5 0.0 copy-start.2
  4.6 0.0 copy-start.7
  4.6 0.0 copy-start.4
  4.6 1.0 %copy.17 = bf16[2,8,1,36,256]{4,0,3,2,1:T(2,128)(2,1)} copy(bf16[2,8,1,36,256]{4,3,1,2,0:T(8,128)(2,1)S(1)} %pad_maximum_fusion) | data formatting | bytes 589824 | tf_op jit(solution)/shard_map/stack | solution.py:25
  5.6 7.3 %all-to-all-start = ((bf16[2,8,1,36,256]{4,0,3,2,1:T(2,128)(2,1)}), bf16[2,8,1,36,256]{4,0,3,2,1:T(2,128)(2,1)S(1)}, u32[]{:S(2)}, u32[]{:S(2)}) async-start(bf16[2,8,1,36,256]{4,0,3,2,1:T(2,128)(2,1)} %copy.17), calls=%async_computation | async-start | bytes 589824 | tf_op jit(solution)/shard_map/all_to_all | solution.py:26
  13.0 0.0 copy-done.3
  13.0 0.6 fusion.11
  14.3 0.0 copy-done.2
  14.3 0.2 fusion.21
  14.5 0.1 fusion.8
  14.7 0.0 copy-done.7
  14.7 0.6 dynamic-slice
  16.0 0.0 copy-done.4
  16.0 0.1 fusion.19
  16.1 0.1 negate_dynamic-update-slice_fusion
  16.2 21.8 %all-reduce.1 = f32[16]{0:T(128)S(1)} all-reduce(f32[16]{0:T(128)S(1)} %negate_dynamic-update-slice_fusion), channel_id=2, replica_groups=mesh['sp'=8,'tp'=4] {'sp'}, use_global_device_ids=true, to_apply=%add.1 | all-reduce | flops 16 | bytes 128
  38.1 2.5 %reduce-window.6 = f32[2,3,128]{2,1,0:T(4,128)S(1)} reduce-window(f32[2,3,128]{2,1,0:T(4,128)S(1)} %reshape.81, f32[]{:T(128)} %constant.42.clone.1), window={size=1x1x128 pad=0_0x0_0x0_127}, to_apply=%region_2.3 | reduce-window | flops 97536 | bytes 6148 | tf_op jit(solution)/shard_map/reduce-window
  40.6 0.1 slice_reduce_fusion
  40.7 0.2 reduce-window.9
  40.9 0.1 slice.21
  40.9 0.1 add_bitcast_fusion
  41.0 0.1 reshape.84
  41.1 0.1 select_reduce_fusion
  41.2 0.1 exponential_bitcast_fusion
  41.3 0.1 fusion.5
  41.4 17.1 %psum.7 = bf16[2,128]{1,0:T(2,128)(2,1)S(1)} all-reduce(f32[2,128]{1,0:T(2,128)S(1)} %bitcast.66), channel_id=1, replica_groups=mesh['sp'=8,'tp'=4] {'sp'}, use_global_device_ids=true, to_apply=%region_6.7 | all-reduce | flops 256 | bytes 1536 | tf_op jit(solution)/shard_map/psum | solution.py:48
  58.5 0.0 collective-permute-start
  58.6 3.0 %collective-permute-done = bf16[256]{0:T(256)(128)(2,1)S(1)} collective-permute-done((bf16[256]{0:T(256)(128)(2,1)S(1)}, bf16[256]{0:T(256)(128)(2,1)S(1)}, u32[]{:S(2)}, u32[]{:S(2)}) %collective-permute-start) | collective-permute-done | bytes 544 | tf_op jit(solution)/shard_map/ppermute | solution.py:53
  61.6 0.0 collective-permute-start.1
  61.6 3.0 %collective-permute-done.1 = bf16[256]{0:T(256)(128)(2,1)S(1)} collective-permute-done((bf16[256]{0:T(256)(128)(2,1)S(1)}, bf16[256]{0:T(256)(128)(2,1)S(1)}, u32[]{:S(2)}, u32[]{:S(2)}) %collective-permute-start.1) | collective-permute-done | bytes 544 | tf_op jit(solution)/shard_map/ppermute | solution.py:53
  64.6 0.0 collective-permute-start.2
  64.6 3.0 %collective-permute-done.2 = bf16[256]{0:T(256)(128)(2,1)S(1)} collective-permute-done((bf16[256]{0:T(256)(128)(2,1)S(1)}, bf16[256]{0:T(256)(128)(2,1)S(1)}, u32[]{:S(2)}, u32[]{:S(2)}) %collective-permute-start.2) | collective-permute-done | bytes 544 | tf_op jit(solution)/shard_map/ppermute | solution.py:53
  67.6 0.2 dynamic-update-slice.1
  67.7 0.2 dynamic-update-slice.2
  67.9 0.2 dynamic-update-slice.3
  68.1 0.2 dynamic-update-slice.4
  68.4 0.2 dynamic-update-slice.5
  68.5 0.2 dynamic-update-slice.6
  68.7 0.2 dynamic-update-slice.7
  68.9 0.2 dynamic-update-slice.8
  69.1 0.7 dynamic_slice.4
  69.8 0.0 all-to-all-done
  69.8 0.4 fusion.20
  70.2 0.8 %copy_bitcast_fusion = (bf16[1,8,36,256]{3,1,2,0:T(8,128)(2,1)}, bf16[1,8,36,256]{3,1,2,0:T(8,128)(2,1)}) fusion(bf16[1,8,1,36,256]{4,0,3,2,1:T(2,128)(2,1)S(1)} %get-tuple-element.11, bf16[1,8,1,36,256]{4,0,3,2,1:T(2,128)(2,1)S(1)} %get-tuple-element.12), kind=kLoop, calls=%fused_computation.14 | loop fusion | bytes 589824 | tf_op jit(solution)/shard_map/squeeze | solution.py:28
  (14 shorter events, 0.2 us)
Async XLA Ops:
  0.6 1.8 %copy-start = (bf16[2048,256]{1,0:T(8,128)(2,1)S(1)}, bf16[2048,256]{1,0:T(8,128)(2,1)}, u32[]{:S(2)}) copy-start(bf16[2048,256]{1,0:T(8,128)(2,1)} %param.11) | copy-start | bytes 3145732
  0.6 1.9 %copy-start.1 = (bf16[288,2048]{1,0:T(8,128)(2,1)S(1)}, bf16[288,2048]{1,0:T(8,128)(2,1)}, u32[]{:S(2)}) copy-start(bf16[288,2048]{1,0:T(8,128)(2,1)} %param.7) | copy-start | bytes 3538948
  2.6 1.3 %copy-start.5 = (f32[2048]{0:T(1024)S(1)}, f32[2048]{0:T(1024)}, u32[]{:S(2)}) copy-start(f32[2048]{0:T(1024)} %param.9) | copy-start | bytes 24580
  2.6 1.3 %copy-start.6 = (bf16[2048,256]{1,0:T(8,128)(2,1)S(1)}, bf16[2048,256]{1,0:T(8,128)(2,1)}, u32[]{:S(2)}) copy-start(bf16[2048,256]{1,0:T(8,128)(2,1)} %param.10) | copy-start | bytes 3145732
  4.5 8.5 %copy-start.3 = (bf16[2048]{0:T(1024)(128)(2,1)S(1)}, bf16[2048]{0:T(1024)(128)(2,1)}, u32[]{:S(2)}) copy-start(bf16[2048]{0:T(1024)(128)(2,1)} %param.8) | copy-start | bytes 12292
  4.5 9.8 %copy-start.2 = (bf16[2048,256]{1,0:T(8,128)(2,1)S(1)}, bf16[2048,256]{1,0:T(8,128)(2,1)}, u32[]{:S(2)}) copy-start(bf16[2048,256]{1,0:T(8,128)(2,1)} %param.12) | copy-start | bytes 3145732
  4.6 10.1 %copy-start.7 = (u32[32]{0:T(128)S(1)}, u32[32]{0:T(128)}, u32[]{:S(2)}) copy-start(u32[32]{0:T(128)} %constant.60) | copy-start | bytes 388
  4.6 11.3 %copy-start.4 = (f32[288,2]{0,1:T(2,128)S(1)}, f32[288,2]{0,1:T(2,128)}, u32[]{:S(2)}) copy-start(f32[288,2]{0,1:T(2,128)} %param.13) | copy-start | bytes 6916
  5.6 64.1 %all-to-all-start = ((bf16[2,8,1,36,256]{4,0,3,2,1:T(2,128)(2,1)}), bf16[2,8,1,36,256]{4,0,3,2,1:T(2,128)(2,1)S(1)}, u32[]{:S(2)}, u32[]{:S(2)}) async-start(bf16[2,8,1,36,256]{4,0,3,2,1:T(2,128)(2,1)} %copy.17), calls=%async_computation | async-start | bytes 589824 | tf_op jit(solution)/shard_map/all_to_all | solution.py:26
  58.5 3.0 %collective-permute-start = (bf16[256]{0:T(256)(128)(2,1)S(1)}, bf16[256]{0:T(256)(128)(2,1)S(1)}, u32[]{:S(2)}, u32[]{:S(2)}) collective-permute-start(bf16[256]{0:T(256)(128)(2,1)S(1)} %bitcast.62), channel_id=1, source_target_pairs={{0,1},{1,2},{2,3},{3,0},{4,5},{5,6},{6,7},{7,4},{8,9},{9,10},{10,1... | collective-permute-start | bytes 1544 | tf_op jit(solution)/shard_map/ppermute | solution.py:53
  61.6 3.0 %collective-permute-start.1 = (bf16[256]{0:T(256)(128)(2,1)S(1)}, bf16[256]{0:T(256)(128)(2,1)S(1)}, u32[]{:S(2)}, u32[]{:S(2)}) collective-permute-start(bf16[256]{0:T(256)(128)(2,1)S(1)} %collective-permute-done), channel_id=1, source_target_pairs={{0,1},{1,2},{2,3},{3,0},{4,5},{5,6},{6,7},{7,4},{8,9},{9,10},{10,1... | collective-permute-start | bytes 1544 | tf_op jit(solution)/shard_map/ppermute | solution.py:53
  64.6 3.0 %collective-permute-start.2 = (bf16[256]{0:T(256)(128)(2,1)S(1)}, bf16[256]{0:T(256)(128)(2,1)S(1)}, u32[]{:S(2)}, u32[]{:S(2)}) collective-permute-start(bf16[256]{0:T(256)(128)(2,1)S(1)} %collective-permute-done.1), channel_id=1, source_target_pairs={{0,1},{1,2},{2,3},{3,0},{4,5},{5,6},{6,7},{7,4},{8,9},{9,10},{10,1... | collective-permute-start | bytes 1544 | tf_op jit(solution)/shard_map/ppermute | solution.py:53
